TPU v7x, 32 devices: a whole 2x2x4 slice. The times are simulated.
32 devices in a mesh: sp: 8 (over z, x), tp: 4 (over y, core).
Axes of the slice: x: 2, y: 2, z: 4, core: 2. Of those that a mesh axis runs over, the one named last changes fastest.
Arguments:
- residual: bfloat16 [2048, 2048], P(('sp', 'tp')), may hold values from -6 to 6
- queries: bfloat16 [2048, 1024], P('sp', 'tp'), may hold values from -8 to 8
- key_pairs: bfloat16 [2048, 512], P('sp', 'tp'), may hold values from -8 to 8
- values: bfloat16 [2048, 512], P('sp', 'tp'), may hold values from -6 to 6
- lambdas: float32 [8], P('tp'), may hold values from 0.3 to 0.8
- head_gain: float32 [128], replicated, may hold values from 0.1 to 1.9
- out_weight: bfloat16 [1024, 2048], replicated, may hold values from -0.1875 to 0.1875
- mixer_gain: float32 [2048], replicated, may hold values from 0.1 to 1.9
- before_gain: float32 [2048], replicated, may hold values from 0.1 to 1.9
- after_gain: float32 [2048], replicated, may hold values from 0.1 to 1.9
- gate_weight: bfloat16 [2048, 5632], P('sp', 'tp'), may hold values from -0.125 to 0.125
- up_weight: bfloat16 [2048, 5632], P('sp', 'tp'), may hold values from -0.125 to 0.125
- down_weight: bfloat16 [5632, 2048], P('tp', 'sp'), may hold values from -0.078125 to 0.078125
Outputs:
- updated: bfloat16 [2048, 2048], P(('sp', 'tp'))
All inputs are finite; a program needn't handle non-finite values.
Results may differ from a plain program's by a relative error of at most 0.014.
Values may be sent and summed in bfloat16 or wider, within the bound.
A program may use at most 128 MiB of HBM per device.

v0:
```python
import math

import jax
import jax.numpy as jnp
from jax import lax
from jax.experimental import pallas as pl
from jax.experimental.pallas import tpu as pltpu
from jax.sharding import PartitionSpec as P

HEAD_DIM = 64


def row_norm(values_in, gain, epsilon):
    mean_square = jnp.mean(values_in * values_in, axis=-1, keepdims=True)
    return values_in * lax.rsqrt(mean_square + epsilon) * gain


def on_device(
    residual,
    queries,
    key_pairs,
    values,
    lambdas,
    head_gain,
    out_weight,
    mixer_gain,
    before_gain,
    after_gain,
    gate_weight,
    up_weight,
    down_weight,
):
    tokens_here = queries.shape[0]
    quarter = residual.shape[0]
    width = 2 * HEAD_DIM
    local_heads = queries.shape[1] // width
    scale = 1.0 / math.sqrt(HEAD_DIM)
    height = local_heads * tokens_here
    query_rows = jnp.transpose(
        queries.reshape(tokens_here, local_heads, 2, HEAD_DIM), (2, 1, 0, 3)
    ).reshape(2, height, HEAD_DIM)
    empty = (
        jnp.full((height,), -1e30, jnp.float32),
        jnp.zeros((height,), jnp.float32),
        jnp.zeros((height, width), jnp.float32),
    )
    state = (empty, empty)
    key_piece = lax.all_gather(key_pairs, "sp", axis=0, tiled=True)
    value_piece = lax.all_gather(values, "sp", axis=0, tiled=True)
    length = key_piece.shape[0]
    span = length
    for split_count in range(1, length + 1):
        if length % split_count == 0 and length // split_count <= 2048:
            span = length // split_count
            break
    key_blocks = key_piece.reshape(length // span, span, 2, HEAD_DIM)
    value_blocks = value_piece.reshape(length // span, span, width)

    def advance(carry, blocks_in):
        key_block, value_block = blocks_in
        renewed = []
        for which in range(2):
            running_top, running_total, running_numer = carry[which]
            score = (
                jnp.dot(
                    query_rows[which], key_block[:, which].T, preferred_element_type=jnp.float32
                )
                * scale
            )
            new_top = jnp.maximum(running_top, jnp.max(score, axis=1))
            shrink = jnp.exp(running_top - new_top)
            expo = jnp.exp(score - new_top[:, None])
            new_total = running_total * shrink + jnp.sum(expo, axis=1)
            new_numer = running_numer * shrink[:, None] + jnp.dot(
                expo.astype(jnp.bfloat16), value_block, preferred_element_type=jnp.float32
            )
            renewed.append((new_top, new_total, new_numer))
        return (tuple(renewed), None)

    state, _ = lax.scan(advance, state, (key_blocks, value_blocks))
    first_map, second_map = state
    lambda_rows = jnp.repeat(lambdas, tokens_here)[:, None]
    attended = first_map[2] / first_map[1][:, None] - lambda_rows * (
        second_map[2] / second_map[1][:, None]
    )
    normed = row_norm(attended, head_gain, 1e-05).astype(jnp.bfloat16)
    head_out = jnp.transpose(normed.reshape(local_heads, tokens_here, width), (1, 0, 2)).reshape(
        tokens_here, local_heads * width
    )
    grouped = head_out.reshape(lax.axis_size("tp"), quarter, local_heads * width)
    mixed = jnp.dot(
        lax.all_to_all(grouped, "tp", split_axis=0, concat_axis=2, tiled=True)[0],
        out_weight,
        preferred_element_type=jnp.float32,
    ).astype(jnp.bfloat16)[None][0]
    stream = residual.astype(jnp.float32) + row_norm(mixed.astype(jnp.float32), mixer_gain, 1e-06)
    normed_in = row_norm(stream, before_gain, 1e-06).astype(jnp.bfloat16)
    gathered = lax.all_gather(normed_in, "tp", axis=0, tiled=True)
    empty_hidden = jnp.zeros((gathered.shape[0], gate_weight.shape[1]), jnp.float32)
    pieces = (
        lax.all_gather(gate_weight, "sp", axis=0, tiled=True),
        lax.all_gather(up_weight, "sp", axis=0, tiled=True),
    )
    columns = lax.slice_in_dim(gathered, 0, pieces[0].shape[0], axis=1)
    gate_part = jnp.dot(columns, pieces[0], preferred_element_type=jnp.float32)
    up_part = jnp.dot(columns, pieces[1], preferred_element_type=jnp.float32)
    gate = empty_hidden + gate_part
    up = empty_hidden + up_part
    down_whole = lax.all_gather(down_weight, "sp", axis=1, tiled=True)
    hidden = (jax.nn.silu(gate) * up).astype(jnp.bfloat16)
    picked = lax.slice_in_dim(hidden, 0, lax.axis_size("tp") * quarter, axis=0)
    channel = lax.psum_scatter(
        jnp.dot(picked, down_whole, preferred_element_type=jnp.float32).astype(jnp.bfloat16),
        "tp",
        scatter_dimension=0,
        tiled=True,
    )
    updated = stream + 0.5 * row_norm(channel.astype(jnp.float32), after_gain, 1e-06)
    return updated.astype(jnp.bfloat16)


MESH = pl.DeviceIdType.MESH


def flip(index, bits):
    bit = 1
    while bit <= bits:
        if bits & bit:
            index = index + bit - 2 * bit * ((index // bit) % 2)
        bit *= 2
    return index


def layer(
    residual,
    queries,
    key_pairs,
    values,
    lambdas,
    head_gain,
    out_weight,
    mixer_gain,
    before_gain,
    after_gain,
    gate_weight,
    up_weight,
    down_in,
    updated,
    gate_in,
    up_in,
    hidden,
    kv,
    gate_w,
    up_w,
    down_w,
    head_out,
    head_in,
    stream,
    x,
    p,
    from_core,
    from_y,
    from_z,
    send_sems,
    recv_sems,
    local_sems,
):
    depth = down_in.shape[0]
    n_tp = head_in.shape[0]
    quarter, width_all = residual.shape
    width = 2 * HEAD_DIM
    heads = queries.shape[1] // width
    place, member = lax.axis_index("sp"), lax.axis_index("tp")
    used = [0]
    copies = []

    def send(src, dst, axis, bits):
        at = used[0]
        used[0] += 1
        target = flip(place if axis == "sp" else member, bits)
        copy = pltpu.make_async_remote_copy(
            src_ref=src,
            dst_ref=dst,
            send_sem=send_sems.at[at],
            recv_sem=recv_sems.at[at],
            device_id={axis: target},
            device_id_type=MESH,
        )
        copy.start()
        copies.append(copy)
        return copy

    partners = [("sp", 1)] + [("sp", 2 * j) for j in range(1, depth)]
    partners += [("tp", j) for j in range(1, n_tp)]
    barrier = pltpu.get_barrier_semaphore()
    for axis, bits in partners:
        target = flip(place if axis == "sp" else member, bits)
        pl.semaphore_signal(barrier, inc=1, device_id={axis: target}, device_id_type=MESH)
    pl.semaphore_wait(barrier, len(partners))

    kv[0, :, :width] = key_pairs[...]
    kv[0, :, width:] = values[...]
    far = send(kv.at[0], kv.at[2], "sp", 4)
    near = send(kv.at[0], kv.at[1], "sp", 2)
    kv_x = [send(kv.at[0], kv.at[depth], "sp", 1)]
    for source, target in ((gate_weight, gate_in), (up_weight, up_in)):
        columns = target.shape[2]
        for j in range(depth):
            target[j] = source[:, j * columns : (j + 1) * columns]
    far.wait_recv()
    relayed = send(kv.at[2], kv.at[3], "sp", 2)
    kv_x.append(send(kv.at[2], kv.at[depth + 2], "sp", 1))

    def scatter(source, target, at):
        mine = source.at[place // 2]
        local = pltpu.make_async_copy(mine, target.at[place], local_sems.at[at])
        local.start()
        over_z = [
            send(source.at[flip(place, 2 * j) // 2], target.at[place], "sp", 2 * j)
            for j in range(1, depth)
        ]
        return local, over_z, send(mine, target.at[place], "sp", 1)

    def forward(target, over_z):
        over_x = []
        for j in range(1, depth):
            over_z[j - 1].wait_recv()
            slot = target.at[flip(place, 2 * j)]
            over_x.append(send(slot, slot, "sp", 1))
        return over_x

    gate_moves = scatter(gate_in, gate_w, 0)
    up_moves = scatter(up_in, up_w, 1)
    for j, copy in ((1, near), (3, relayed)):
        copy.wait_recv()
        kv_x.append(send(kv.at[j], kv.at[depth + j], "sp", 1))
    for copy in kv_x:
        copy.wait_recv()

    def attend(tile, _):
        rows = pl.ds(pl.multiple_of(tile * quarter, quarter), quarter)
        for h in range(heads):
            parts = []
            for which in range(2):
                start = (2 * h + which) * HEAD_DIM
                query = queries[rows, start : start + HEAD_DIM]
                keys = kv[:, :, which * HEAD_DIM : (which + 1) * HEAD_DIM]
                keys = keys.reshape(2 * depth * keys.shape[1], HEAD_DIM)
                score = lax.dot_general(
                    query, keys, (((1,), (1,)), ((), ())), preferred_element_type=jnp.float32
                ) * (1.0 / math.sqrt(HEAD_DIM))
                expo = jnp.exp(score - jnp.max(score, axis=1, keepdims=True))
                total = jnp.sum(expo, axis=1, keepdims=True)
                vals = kv[:, :, width : 2 * width]
                vals = vals.reshape(2 * depth * vals.shape[1], width)
                numer = jnp.dot(
                    expo.astype(jnp.bfloat16), vals, preferred_element_type=jnp.float32
                )
                parts.append(numer / total)
            attended = parts[0] - lambdas[h] * parts[1]
            normed = row_norm(attended, head_gain[...], 1e-05).astype(jnp.bfloat16)
            head_out[tile, :, h * width : (h + 1) * width] = normed
        return 0

    lax.fori_loop(0, n_tp, attend, 0)
    moved = [send(head_out.at[flip(member, j)], head_in.at[member], "tp", j) for j in range(1, n_tp)]
    head_in[member] = head_out[member]
    gate_x = forward(gate_w, gate_moves[1])
    for copy in moved:
        copy.wait_recv()
    step = head_in.shape[2]
    mixed = jnp.zeros((quarter, width_all), jnp.float32)
    for m in range(n_tp):
        mixed = mixed + jnp.dot(
            head_in[m], out_weight[m * step : (m + 1) * step], preferred_element_type=jnp.float32
        )
    mixed = mixed.astype(jnp.bfloat16).astype(jnp.float32)
    stream[...] = residual[...].astype(jnp.float32) + row_norm(mixed, mixer_gain[...], 1e-06)
    x[0] = row_norm(stream[...], before_gain[...], 1e-06).astype(jnp.bfloat16)

    half = 2 * depth
    far = send(x.at[0], x.at[2], "sp", 4)
    near = send(x.at[0], x.at[1], "sp", 2)
    x_c = [send(x.at[0], x.at[half], "tp", 1)]
    x_y = [send(x.at[0], x.at[depth], "tp", 2)]
    up_x = forward(up_w, up_moves[1])
    far.wait_recv()
    relayed = send(x.at[2], x.at[3], "sp", 2)
    down_moves = scatter(down_in, down_w, 2)
    order = ((2, far), (1, near), (3, relayed))
    for j, copy in order:
        if j != 2:
            copy.wait_recv()
        x_y.append(send(x.at[j], x.at[depth + j], "tp", 2))
        x_c.append(send(x.at[j], x.at[half + j], "tp", 1))
    for local, _, over_x in (gate_moves, up_moves):
        local.wait()
        over_x.wait_recv()
    for copy in gate_x + up_x:
        copy.wait_recv()

    blocks = gate_w.shape[0]
    units = gate_w.shape[2]
    span = down_w.shape[2]

    def widen(tile, _):
        rows = x[pl.ds(2 * tile, 2)].reshape(2 * quarter, width_all)
        gate = jnp.dot(
            rows, gate_w[...].reshape(width_all, units), preferred_element_type=jnp.float32
        )
        up = jnp.dot(rows, up_w[...].reshape(width_all, units), preferred_element_type=jnp.float32)
        hidden[tile] = (gate / (1.0 + jnp.exp(-gate)) * up).astype(jnp.bfloat16)
        return 0

    def narrow(tile, _):
        for m in range(blocks):
            part = jnp.dot(hidden[tile], down_w[m], preferred_element_type=jnp.float32)
            p[pl.ds(2 * tile, 2), :, m * span : (m + 1) * span] = part.astype(
                jnp.bfloat16
            ).reshape(2, quarter, span)
        return 0

    def group(at, body):
        lax.fori_loop(at * depth // 2, (at + 1) * depth // 2, body, 0)

    group(0, widen)
    x_last = []
    for j, copy in zip((0, 2, 1, 3), x_y):
        copy.wait_recv()
        x_last.append(send(x.at[depth + j], x.at[half + depth + j], "tp", 1))
    down_x = forward(down_w, down_moves[1])
    for copy in x_c:
        copy.wait_recv()
    group(2, widen)
    group(1, widen)
    for copy in x_last:
        copy.wait_recv()
    group(3, widen)
    down_moves[0].wait()
    down_moves[2].wait_recv()
    for copy in down_x:
        copy.wait_recv()
    group(3, narrow)
    r_d = [send(p.at[half + depth + j], from_core.at[depth + j], "tp", 1) for j in range(depth)]
    group(1, narrow)
    r_y = []
    turns = (3, 1, 2, 0)
    for j in turns:
        r_d[j].wait_recv()
        p[depth + j] = (
            p[depth + j].astype(jnp.float32) + from_core[depth + j].astype(jnp.float32)
        ).astype(jnp.bfloat16)
        r_y.append(send(p.at[depth + j], from_y.at[j], "tp", 2))
    group(2, narrow)
    r_c = [send(p.at[half + j], from_core.at[j], "tp", 1) for j in range(depth)]
    group(0, narrow)
    r_z = []
    for copy, j in zip(r_y, turns):
        r_c[j].wait_recv()
        copy.wait_recv()
        total = (
            p[j].astype(jnp.float32)
            + from_core[j].astype(jnp.float32)
            + from_y[j].astype(jnp.float32)
        )
        if j == 2:
            r_z[0].wait_recv()
            total = total + from_z[2].astype(jnp.float32)
        if j:
            p[j] = total.astype(jnp.bfloat16)
            r_z.append(send(p.at[j], from_z.at[j - 1], "sp", 4 if j == 2 else 2))
    for copy, slot in ((r_z[1], 0), (r_z[2], 1)):
        copy.wait_recv()
        total = total + from_z[slot].astype(jnp.float32)
    channel = total.astype(jnp.bfloat16).astype(jnp.float32)
    updated[...] = (stream[...] + 0.5 * row_norm(channel, after_gain[...], 1e-06)).astype(
        updated.dtype
    )
    for copy in copies:
        copy.wait_send()


def one_kernel(
    residual,
    queries,
    key_pairs,
    values,
    lambdas,
    head_gain,
    out_weight,
    mixer_gain,
    before_gain,
    after_gain,
    gate_weight,
    up_weight,
    down_weight,
):
    n_sp, n_tp = lax.axis_size("sp"), lax.axis_size("tp")
    depth = n_sp // 2
    quarter, width_all = residual.shape
    tokens_here, query_width = queries.shape
    inner, units_all = gate_weight.shape
    units = units_all // depth
    span = down_weight.shape[1]
    down_in = down_weight.reshape(depth, units, span)
    tiles = 4 * depth
    total_sends = 7 * (depth - 1) + 4 + 3 + 3 * depth - 3 + n_tp - 1 + 2 * tiles
    vmem = pl.BlockSpec(memory_space=pltpu.VMEM)
    hbm = pl.BlockSpec(memory_space=pl.ANY)
    smem = pl.BlockSpec(memory_space=pltpu.SMEM)
    bf16 = jnp.bfloat16
    return pl.pallas_call(
        layer,
        out_shape=jax.ShapeDtypeStruct(residual.shape, bf16),
        in_specs=[vmem] * 4 + [smem] + [vmem] * 7 + [hbm],
        out_specs=vmem,
        scratch_shapes=[
            pltpu.VMEM((depth, inner, units), bf16),
            pltpu.VMEM((depth, inner, units), bf16),
            pltpu.VMEM((tiles // 2, 2 * quarter, units), bf16),
            pltpu.VMEM((n_sp, tokens_here, 2 * key_pairs.shape[1]), bf16),
            pltpu.VMEM((n_sp, inner, units), bf16),
            pltpu.VMEM((n_sp, inner, units), bf16),
            pltpu.VMEM((n_sp, units, span), bf16),
            pltpu.VMEM((n_tp, quarter, query_width), bf16),
            pltpu.VMEM((n_tp, quarter, query_width), bf16),
            pltpu.VMEM((quarter, width_all), jnp.float32),
            pltpu.VMEM((tiles, quarter, width_all), bf16),
            pltpu.VMEM((tiles, quarter, width_all), bf16),
            pltpu.VMEM((2 * depth, quarter, width_all), bf16),
            pltpu.VMEM((depth, quarter, width_all), bf16),
            pltpu.VMEM((depth - 1, quarter, width_all), bf16),
            pltpu.SemaphoreType.DMA((total_sends,)),
            pltpu.SemaphoreType.DMA((total_sends,)),
            pltpu.SemaphoreType.DMA((3,)),
        ],
        compiler_params=pltpu.CompilerParams(
            collective_id=0, has_side_effects=True, vmem_limit_bytes=60 * 1024 * 1024
        ),
    )(
        residual,
        queries,
        key_pairs,
        values,
        lambdas,
        head_gain[None],
        out_weight,
        mixer_gain[None],
        before_gain[None],
        after_gain[None],
        gate_weight,
        up_weight,
        down_in,
    )


def fits(mesh):
    return mesh.shape["tp"] == 4 and mesh.shape["sp"] == 8


def solution(mesh):
    return jax.shard_map(
        one_kernel if fits(mesh) else on_device,
        mesh=mesh,
        in_specs=(
            P(("sp", "tp"), None),
            P("sp", "tp"),
            P("sp", "tp"),
            P("sp", "tp"),
            P("tp"),
            P(),
            P(),
            P(),
            P(),
            P(),
            P("sp", "tp"),
            P("sp", "tp"),
            P("tp", "sp"),
        ),
        out_specs=P(("sp", "tp"), None),
        check_vma=False,
    )
```

profile of v0, /device:TPU:5, one launch (start us, length us, event | category | flops | bytes accessed | tf_op | source)
XLA Modules:
  0.0 124.2 jit_solution(6989869318159038939)
XLA Ops:
  0.0 122.5 %shard_map.127 = bf16[64,2048]{1,0:T(8,128)(2,1)} custom-call(bf16[64,2048]{1,0:T(8,128)(2,1)} %residual.1, bf16[256,256]{1,0:T(8,128)(2,1)} %queries.1, bf16[256,128]{1,0:T(8,128)(2,1)} %key_pairs.1, bf16[256,128]{1,0:T(8,128)(2,1)} %values.1, f32[2]{0:T(128)} %lambdas.1, f32[1,128]{1,0:T(1,128)} %bitcast.9, bf16[1024,2048]{1,0:T(8,128)(2,1)} %out_weight.1, ...), custom_call_target="tpu_custom_call" | custom-call | tf_op jit(solution)/shard_map/pallas_call | solution.py:412
  122.5 1.7 %copy.15 = bf16[64,2048]{1,0:T(8,128)(2,1)} copy(bf16[64,2048]{1,0:T(8,128)(2,1)} %shard_map.127) | data formatting | bytes 524288
where the time goes:
time: 124 us
  Pallas kernels  123 us (99%)
  local copies, waits for them, and re-layouts  1.67 us (1%)
    pallas_call x1, Pallas kernels, one_kernel(): pl.pallas_call(layer, out_shape=jax.ShapeDtypeStruct(residual.shape, bf16...  123 us

commit v1 on v0

v1 whole, which is shorter than its diff:
```python
import math

import jax
import jax.numpy as jnp
from jax import lax
from jax.experimental import pallas as pl
from jax.experimental.pallas import tpu as pltpu
from jax.sharding import PartitionSpec as P

HEAD_DIM = 64


def row_norm(values_in, gain, epsilon):
    mean_square = jnp.mean(values_in * values_in, axis=-1, keepdims=True)
    return values_in * lax.rsqrt(mean_square + epsilon) * gain


def on_device(
    residual,
    queries,
    key_pairs,
    values,
    lambdas,
    head_gain,
    out_weight,
    mixer_gain,
    before_gain,
    after_gain,
    gate_weight,
    up_weight,
    down_weight,
):
    tokens_here = queries.shape[0]
    quarter = residual.shape[0]
    width = 2 * HEAD_DIM
    local_heads = queries.shape[1] // width
    scale = 1.0 / math.sqrt(HEAD_DIM)
    height = local_heads * tokens_here
    query_rows = jnp.transpose(
        queries.reshape(tokens_here, local_heads, 2, HEAD_DIM), (2, 1, 0, 3)
    ).reshape(2, height, HEAD_DIM)
    empty = (
        jnp.full((height,), -1e30, jnp.float32),
        jnp.zeros((height,), jnp.float32),
        jnp.zeros((height, width), jnp.float32),
    )
    state = (empty, empty)
    key_piece = lax.all_gather(key_pairs, "sp", axis=0, tiled=True)
    value_piece = lax.all_gather(values, "sp", axis=0, tiled=True)
    length = key_piece.shape[0]
    span = length
    for split_count in range(1, length + 1):
        if length % split_count == 0 and length // split_count <= 2048:
            span = length // split_count
            break
    key_blocks = key_piece.reshape(length // span, span, 2, HEAD_DIM)
    value_blocks = value_piece.reshape(length // span, span, width)

    def advance(carry, blocks_in):
        key_block, value_block = blocks_in
        renewed = []
        for which in range(2):
            running_top, running_total, running_numer = carry[which]
            score = (
                jnp.dot(
                    query_rows[which], key_block[:, which].T, preferred_element_type=jnp.float32
                )
                * scale
            )
            new_top = jnp.maximum(running_top, jnp.max(score, axis=1))
            shrink = jnp.exp(running_top - new_top)
            expo = jnp.exp(score - new_top[:, None])
            new_total = running_total * shrink + jnp.sum(expo, axis=1)
            new_numer = running_numer * shrink[:, None] + jnp.dot(
                expo.astype(jnp.bfloat16), value_block, preferred_element_type=jnp.float32
            )
            renewed.append((new_top, new_total, new_numer))
        return (tuple(renewed), None)

    state, _ = lax.scan(advance, state, (key_blocks, value_blocks))
    first_map, second_map = state
    lambda_rows = jnp.repeat(lambdas, tokens_here)[:, None]
    attended = first_map[2] / first_map[1][:, None] - lambda_rows * (
        second_map[2] / second_map[1][:, None]
    )
    normed = row_norm(attended, head_gain, 1e-05).astype(jnp.bfloat16)
    head_out = jnp.transpose(normed.reshape(local_heads, tokens_here, width), (1, 0, 2)).reshape(
        tokens_here, local_heads * width
    )
    grouped = head_out.reshape(lax.axis_size("tp"), quarter, local_heads * width)
    mixed = jnp.dot(
        lax.all_to_all(grouped, "tp", split_axis=0, concat_axis=2, tiled=True)[0],
        out_weight,
        preferred_element_type=jnp.float32,
    ).astype(jnp.bfloat16)[None][0]
    stream = residual.astype(jnp.float32) + row_norm(mixed.astype(jnp.float32), mixer_gain, 1e-06)
    normed_in = row_norm(stream, before_gain, 1e-06).astype(jnp.bfloat16)
    gathered = lax.all_gather(normed_in, "tp", axis=0, tiled=True)
    empty_hidden = jnp.zeros((gathered.shape[0], gate_weight.shape[1]), jnp.float32)
    pieces = (
        lax.all_gather(gate_weight, "sp", axis=0, tiled=True),
        lax.all_gather(up_weight, "sp", axis=0, tiled=True),
    )
    columns = lax.slice_in_dim(gathered, 0, pieces[0].shape[0], axis=1)
    gate_part = jnp.dot(columns, pieces[0], preferred_element_type=jnp.float32)
    up_part = jnp.dot(columns, pieces[1], preferred_element_type=jnp.float32)
    gate = empty_hidden + gate_part
    up = empty_hidden + up_part
    down_whole = lax.all_gather(down_weight, "sp", axis=1, tiled=True)
    hidden = (jax.nn.silu(gate) * up).astype(jnp.bfloat16)
    picked = lax.slice_in_dim(hidden, 0, lax.axis_size("tp") * quarter, axis=0)
    channel = lax.psum_scatter(
        jnp.dot(picked, down_whole, preferred_element_type=jnp.float32).astype(jnp.bfloat16),
        "tp",
        scatter_dimension=0,
        tiled=True,
    )
    updated = stream + 0.5 * row_norm(channel.astype(jnp.float32), after_gain, 1e-06)
    return updated.astype(jnp.bfloat16)


MESH = pl.DeviceIdType.MESH


def flip(index, bits):
    bit = 1
    while bit <= bits:
        if bits & bit:
            index = index + bit - 2 * bit * ((index // bit) % 2)
        bit *= 2
    return index


PIECES = 2


def layer(
    residual_in,
    queries_in,
    key_in,
    value_in,
    lambdas,
    head_gain,
    out_in,
    mixer_gain,
    before_gain,
    after_gain,
    gate_all,
    up_all,
    down_in,
    updated,
    residual,
    queries,
    out_weight,
    gate_raw,
    up_raw,
    gate_in,
    up_in,
    hidden,
    gate_sum,
    up_sum,
    kv,
    rows_q,
    tops,
    numers,
    gate_w,
    up_w,
    down_w,
    head_out,
    head_in,
    mixed,
    stream,
    x,
    p,
    from_core,
    from_y,
    from_low,
    from_high,
    send_sems,
    recv_sems,
    local_sems,
):
    depth = down_in.shape[0]
    n_tp = head_in.shape[0]
    quarter, width_all = residual.shape
    width = 2 * HEAD_DIM
    heads = queries.shape[1] // width
    tokens_here = queries.shape[0]
    place, member = lax.axis_index("sp"), lax.axis_index("tp")
    used = [0]
    copies = []

    def send(src, dst, axis, bits):
        at = used[0]
        used[0] += 1
        target = flip(place if axis == "sp" else member, bits)
        copy = pltpu.make_async_remote_copy(
            src_ref=src,
            dst_ref=dst,
            send_sem=send_sems.at[at],
            recv_sem=recv_sems.at[at],
            device_id={axis: target},
            device_id_type=MESH,
        )
        copy.start()
        copies.append(copy)
        return copy

    partners = [("sp", 1)] + [("sp", 2 * j) for j in range(1, depth)]
    partners += [("tp", j) for j in range(1, n_tp)]
    barrier = pltpu.get_barrier_semaphore()
    for axis, bits in partners:
        target = flip(place if axis == "sp" else member, bits)
        pl.semaphore_signal(barrier, inc=1, device_id={axis: target}, device_id_type=MESH)

    fetches = []
    for src, dst in (
        (key_in, kv.at[0, :, pl.ds(0, width)]),
        (value_in, kv.at[0, :, pl.ds(width, width)]),
        (queries_in, queries),
        (gate_all, gate_raw),
        (up_all, up_raw),
        (residual_in, residual),
        (out_in, out_weight),
    ):
        fetch = pltpu.make_async_copy(src, dst, local_sems.at[3 + len(fetches)])
        fetch.start()
        fetches.append(fetch)
    fetches[0].wait()
    fetches[1].wait()
    pl.semaphore_wait(barrier, len(partners))

    near = send(kv.at[0], kv.at[1], "sp", 2)
    far = send(kv.at[0], kv.at[2], "sp", 4)
    kv_x = [send(kv.at[0], kv.at[depth], "sp", 1)]

    fetches[2].wait()
    lane = lax.broadcasted_iota(jnp.int32, (tokens_here, width), 1)
    for h in range(heads):
        both = queries[:, h * width : (h + 1) * width].astype(jnp.float32) * (
            1.0 / math.sqrt(HEAD_DIM)
        )
        for which in range(2):
            inside = (lane < HEAD_DIM) if which == 0 else (lane >= HEAD_DIM)
            rows_q[2 * h + which] = jnp.where(inside, both, 0.0).astype(jnp.bfloat16)
    for source, target, fetch in ((gate_raw, gate_in, fetches[3]), (up_raw, up_in, fetches[4])):
        fetch.wait()
        columns = target.shape[2]
        for j in range(depth):
            target[j] = source[:, j * columns : (j + 1) * columns]

    def attend(slots, first):
        keys = jnp.concatenate([kv[slot, :, :width] for slot in slots], axis=0)
        vals = jnp.concatenate([kv[slot, :, width:] for slot in slots], axis=0)
        vals = jnp.concatenate([vals, jnp.ones_like(vals)], axis=1)

        def unit(u, _):
            score = lax.dot_general(
                rows_q[u], keys, (((1,), (1,)), ((), ())), preferred_element_type=jnp.float32
            )
            top = jnp.max(score, axis=1, keepdims=True)
            if not first:
                old = tops[u][:, :1]
                top = jnp.maximum(old, top)
            expo = jnp.exp(score - top).astype(jnp.bfloat16)
            numer = jnp.dot(expo, vals, preferred_element_type=jnp.float32)
            if not first:
                numer = numers[u] * jnp.exp(old - top) + numer
            numers[u] = numer
            tops[u] = jnp.broadcast_to(top, tops.shape[1:])
            return 0

        for u in range(2 * heads):
            unit(u, 0)

    kv_x[0].wait_recv()
    attend((0, depth), True)
    lane_x, low = place % 2, place // 2
    upper = low // 2
    inner = (upper + low % 2) % 2
    mirror = 1 - inner
    pairs = [(j, flip(place, 2 * j) // 2) for j in range(1, depth)]
    crossing = [(2 + inner, 2 - upper), (2 + mirror, 3 - 3 * upper)]

    def plan_z(source, target):
        base = used[0]
        used[0] += (depth - 1) * PIECES
        rows = target.shape[1] // PIECES

        def move(j, goal, k):
            at = base + (j - 1) * PIECES + k
            part = pl.ds(k * rows, rows)
            return pltpu.make_async_remote_copy(
                src_ref=source.at[goal, part],
                dst_ref=target.at[place, part],
                send_sem=send_sems.at[at],
                recv_sem=recv_sems.at[at],
                device_id={"sp": 2 * goal + lane_x},
                device_id_type=MESH,
            )

        def begin(order):
            for j, goal in order:
                for k in range(PIECES):
                    move(j, goal, k).start()

        moves = {(j, k): move(j, goal, k) for j, goal in pairs for k in range(PIECES)}
        copies.extend(moves.values())
        return moves, begin

    def scatter_x(source, target, at):
        mine = source.at[place // 2]
        local = pltpu.make_async_copy(mine, target.at[place], local_sems.at[at])
        local.start()
        return local, send(mine, target.at[place], "sp", 1)

    def forward(target, over_z, j):
        rows = target.shape[1] // PIECES
        over_x = []
        for k in range(PIECES):
            over_z[j, k].wait_recv()
            slot = target.at[flip(place, 2 * j), pl.ds(k * rows, rows)]
            over_x.append(send(slot, slot, "sp", 1))
        return over_x

    def arrived(group):
        for copy in group:
            copy.wait_recv()

    near.wait_recv()
    kv_x.append(send(kv.at[1], kv.at[depth + 1], "sp", 1))
    far.wait_recv()
    relayed = send(kv.at[2], kv.at[3], "sp", 2)
    kv_x.append(send(kv.at[2], kv.at[depth + 2], "sp", 1))
    gate_z, begin_gate = plan_z(gate_in, gate_w)
    begin_gate(crossing[:1])
    kv_x[1].wait_recv()
    attend((1, depth + 1), False)
    relayed.wait_recv()
    kv_x.append(send(kv.at[3], kv.at[depth + 3], "sp", 1))
    begin_gate(crossing[1:] + pairs[:1])
    gate_own = scatter_x(gate_in, gate_w, 0)
    kv_x[2].wait_recv()
    attend((2, depth + 2), False)
    kv_x[3].wait_recv()
    attend((3, depth + 3), False)

    for h in range(heads):
        parts = []
        for which in range(2):
            whole = numers[2 * h + which]
            parts.append(whole[:, :width] / whole[:, width:])
        attended = parts[0] - lambdas[h] * parts[1]
        normed = row_norm(attended, head_gain[...], 1e-05).astype(jnp.bfloat16)
        for t in range(n_tp):
            head_out[t, :, h * width : (h + 1) * width] = normed[t * quarter : (t + 1) * quarter]
    moved = [send(head_out.at[flip(member, j)], head_in.at[member], "tp", j) for j in range(1, n_tp)]
    head_in[member] = head_out[member]
    fetches[5].wait()
    fetches[6].wait()
    step = head_in.shape[2]

    def project(m):
        rows = pl.ds(pl.multiple_of(m * step, step), step)
        return jnp.dot(head_in[m], out_weight[rows], preferred_element_type=jnp.float32)

    mixed[...] = project(member)
    for j, copy in zip(range(1, n_tp), moved):
        copy.wait_recv()
        mixed[...] += project(flip(member, j))
    rounded = mixed[...].astype(jnp.bfloat16).astype(jnp.float32)
    stream[...] = residual[...].astype(jnp.float32) + row_norm(rounded, mixer_gain[...], 1e-06)
    x[0] = row_norm(stream[...], before_gain[...], 1e-06).astype(jnp.bfloat16)

    half = 2 * depth
    bands = [pl.ds(k * (quarter // PIECES), quarter // PIECES) for k in range(PIECES)]

    def send_tile(origin, goal, axis, bits):
        return [send(x.at[origin, band], x.at[goal, band], axis, bits) for band in bands]

    def relay_tile(arriving, origin, *routes):
        moves = [[] for _ in routes]
        for copy, band in zip(arriving, bands):
            copy.wait_recv()
            for route, made in zip(routes, moves):
                goal, axis, bits = route
                made.append(send(x.at[origin, band], x.at[goal, band], axis, bits))
        return moves

    near = send_tile(0, 1, "sp", 2)
    far = send_tile(0, 2, "sp", 4)
    x_c = [send_tile(0, half, "tp", 1)]
    x_y = [send_tile(0, depth, "tp", 2)]
    gate_x = [forward(gate_w, gate_z, j) for j in (1, 2, 3)]
    up_own = scatter_x(up_in, up_w, 1)
    for made, group in zip(
        relay_tile(near, 1, (depth + 1, "tp", 2), (half + 1, "tp", 1)), (x_y, x_c)
    ):
        group.append(made)
    relayed, made_y, made_c = relay_tile(
        far, 2, (3, "sp", 2), (depth + 2, "tp", 2), (half + 2, "tp", 1)
    )
    x_y.append(made_y)
    x_c.append(made_c)
    up_z, begin_up = plan_z(up_in, up_w)
    begin_up(crossing[:1])
    for made, group in zip(
        relay_tile(relayed, 3, (depth + 3, "tp", 2), (half + 3, "tp", 1)), (x_y, x_c)
    ):
        group.append(made)
    begin_up(pairs[:1] + crossing[1:])
    down_z, begin_down = plan_z(down_in, down_w)
    begin_down(crossing[:1])
    down_own = scatter_x(down_in, down_w, 2)

    units = gate_w.shape[2]
    span = down_w.shape[2]
    inner_rows = gate_w.shape[1]
    rows_group = depth * quarter

    def source_of(j):
        return low if j == 0 else flip(place, 2 * j) // 2

    def multiply(w, total, j, g, first):
        begin = 2 * source_of(j)
        columns = pl.ds(pl.multiple_of(begin * inner_rows, 2 * inner_rows), 2 * inner_rows)
        rows = x[g * depth : (g + 1) * depth, :, columns].reshape(rows_group, 2 * inner_rows)
        weights = w[pl.ds(begin, 2)].reshape(2 * inner_rows, units)
        part = jnp.dot(rows, weights, preferred_element_type=jnp.float32)
        total[g] = part if first else total[g] + part

    def multiply_all(w, total, g, sources):
        for j in sources:
            multiply(w, total, j, g, j == 0)

    def finish_hidden(g):
        gate, up = gate_sum[g], up_sum[g]
        hidden[g] = (gate / (1.0 + jnp.exp(-gate)) * up).astype(jnp.bfloat16)

    gate_own[0].wait()
    gate_own[1].wait_recv()
    for group in gate_x:
        arrived(group)
    multiply_all(gate_w, gate_sum, 0, range(depth))
    x_last = []

    def pass_on(j):
        x_last.extend(relay_tile(x_y[j], depth + j, (half + depth + j, "tp", 1)))

    pass_on(0)
    pass_on(1)
    up_x = [forward(up_w, up_z, 1)]
    for group in x_c:
        arrived(group)
    multiply_all(gate_w, gate_sum, 2, range(depth))
    pass_on(2)
    up_x.append(forward(up_w, up_z, 2))
    pass_on(3)
    up_x.append(forward(up_w, up_z, 3))
    begin_down(pairs[:1] + crossing[1:])
    multiply_all(gate_w, gate_sum, 1, range(depth))
    up_own[0].wait()
    up_own[1].wait_recv()
    for g in (0, 1, 2):
        multiply_all(up_w, up_sum, g, (0,))
    for group in x_last:
        arrived(group)
    multiply_all(gate_w, gate_sum, 3, range(depth))
    multiply_all(up_w, up_sum, 3, (0,))
    arrived(up_x[0])
    for g in range(4):
        multiply_all(up_w, up_sum, g, (1,))
    arrived(up_x[1])
    for g in range(4):
        multiply_all(up_w, up_sum, g, (2,))
    arrived(up_x[2])
    for g in range(4):
        multiply_all(up_w, up_sum, g, (3,))
        finish_hidden(g)
    down_own[0].wait()

    def block_of(j, m):
        return 2 * source_of(j) + (lane_x if m == 0 else 1 - lane_x)

    def narrow(j, m, g):
        part = jnp.dot(hidden[g], down_w[block_of(j, m)], preferred_element_type=jnp.float32)
        p[j, m, g * depth : (g + 1) * depth] = part.astype(jnp.bfloat16).reshape(
            depth, quarter, span
        )

    core_y, core_own, over_y, over_low, over_high = {}, {}, {}, {}, {}

    def narrow_all(j, m):
        at = j, m
        narrow(j, m, 3)
        core_y[at] = send(
            p.at[j, m, pl.ds(3 * depth, depth)], from_core.at[j, m, pl.ds(depth, depth)], "tp", 1
        )
        narrow(j, m, 1)
        narrow(j, m, 2)
        core_own[at] = send(
            p.at[j, m, pl.ds(2 * depth, depth)], from_core.at[j, m, pl.ds(0, depth)], "tp", 1
        )
        narrow(j, m, 0)

    def send_y(j, m):
        at = j, m
        core_y[at].wait_recv()
        p[j, m, depth : 2 * depth] = (
            p[j, m, depth : 2 * depth].astype(jnp.float32)
            + from_core[j, m, depth : 2 * depth].astype(jnp.float32)
        ).astype(jnp.bfloat16)
        over_y[at] = send(p.at[j, m, pl.ds(depth, depth)], from_y.at[j, m], "tp", 2)

    def sum_y(j, m):
        at = j, m
        core_own[at].wait_recv()
        over_y[at].wait_recv()
        p[j, m, :depth] = (
            p[j, m, :depth].astype(jnp.float32)
            + from_core[j, m, :depth].astype(jnp.float32)
            + from_y[j, m].astype(jnp.float32)
        ).astype(jnp.bfloat16)
        over_low[at] = [
            send(p.at[j, m, t], from_low.at[j ^ 1, m, t // 2], "sp", 2) for t in (3, 1)
        ]

    def sum_low(j, m):
        for copy in over_low[j ^ 1, m]:
            copy.wait_recv()
        p[j, m, 2] = (
            p[j, m, 2].astype(jnp.float32) + from_low[j, m, 1].astype(jnp.float32)
        ).astype(jnp.bfloat16)
        over_high[j, m] = send(p.at[j, m, 2], from_high.at[j ^ 2, m], "sp", 4)

    def sum_high(j, m):
        over_high[j ^ 2, m].wait_recv()
        columns = pl.ds(pl.multiple_of(block_of(j, m) * span, span), span)
        mixed[:, columns] = (
            p[j, m, 0].astype(jnp.float32)
            + from_low[j, m, 0].astype(jnp.float32)
            + from_high[j, m].astype(jnp.float32)
        )

    down_x = [forward(down_w, down_z, 1)]
    narrow_all(0, 0)
    down_own[1].wait_recv()
    narrow_all(0, 1)
    send_y(0, 0)
    narrow_all(1, 0)
    send_y(0, 1)
    arrived(down_x[0])
    narrow_all(1, 1)
    send_y(1, 0)
    down_x.append(forward(down_w, down_z, 2))
    send_y(1, 1)
    narrow_all(2, 0)
    sum_y(0, 0)
    down_x.append(forward(down_w, down_z, 3))
    send_y(2, 0)
    narrow_all(3, 0)
    sum_y(0, 1)
    arrived(down_x[1])
    narrow_all(2, 1)
    send_y(3, 0)
    arrived(down_x[2])
    narrow_all(3, 1)
    send_y(2, 1)
    sum_y(1, 0)
    send_y(3, 1)
    sum_y(1, 1)
    sum_y(2, 0)
    sum_low(0, 0)
    sum_low(1, 0)
    sum_y(3, 0)
    sum_low(0, 1)
    sum_low(1, 1)
    sum_y(2, 1)
    sum_y(3, 1)
    sum_low(2, 0)
    sum_low(3, 0)
    sum_low(2, 1)
    sum_low(3, 1)
    for j in range(depth):
        sum_high(j, 0)
    for j in range(depth):
        sum_high(j, 1)
    channel = mixed[...].astype(jnp.bfloat16).astype(jnp.float32)
    updated[...] = (stream[...] + 0.5 * row_norm(channel, after_gain[...], 1e-06)).astype(
        updated.dtype
    )
    for copy in copies:
        copy.wait_send()


def one_kernel(
    residual,
    queries,
    key_pairs,
    values,
    lambdas,
    head_gain,
    out_weight,
    mixer_gain,
    before_gain,
    after_gain,
    gate_weight,
    up_weight,
    down_weight,
):
    n_sp, n_tp = lax.axis_size("sp"), lax.axis_size("tp")
    depth = n_sp // 2
    quarter, width_all = residual.shape
    tokens_here, query_width = queries.shape
    width = 2 * HEAD_DIM
    maps = query_width // HEAD_DIM
    inner, units_all = gate_weight.shape
    units = units_all // depth
    span = down_weight.shape[1]
    down_in = down_weight.reshape(depth, units, span)
    tiles = 4 * depth
    weight_sends = 3 * (1 + 2 * (depth - 1) * PIECES)
    tile_sends = (depth - 1 + 3 * depth) * PIECES
    total_sends = 2 * depth - 1 + tile_sends + weight_sends + n_tp - 1 + 12 * depth
    vmem = pl.BlockSpec(memory_space=pltpu.VMEM)
    hbm = pl.BlockSpec(memory_space=pl.ANY)
    smem = pl.BlockSpec(memory_space=pltpu.SMEM)
    bf16 = jnp.bfloat16
    f32 = jnp.float32
    return pl.pallas_call(
        layer,
        out_shape=jax.ShapeDtypeStruct(residual.shape, bf16),
        in_specs=[hbm] * 4 + [smem, vmem, hbm] + [vmem] * 3 + [hbm] * 3,
        out_specs=vmem,
        scratch_shapes=[
            pltpu.VMEM(residual.shape, bf16),
            pltpu.VMEM(queries.shape, bf16),
            pltpu.VMEM(out_weight.shape, bf16),
            pltpu.VMEM(gate_weight.shape, bf16),
            pltpu.VMEM(up_weight.shape, bf16),
            pltpu.VMEM((depth, inner, units), bf16),
            pltpu.VMEM((depth, inner, units), bf16),
            pltpu.VMEM((4, depth * quarter, units), bf16),
            pltpu.VMEM((4, depth * quarter, units), f32),
            pltpu.VMEM((4, depth * quarter, units), f32),
            pltpu.VMEM((n_sp, tokens_here, 2 * key_pairs.shape[1]), bf16),
            pltpu.VMEM((maps, tokens_here, width), bf16),
            pltpu.VMEM((maps, tokens_here, width), f32),
            pltpu.VMEM((maps, tokens_here, 2 * width), f32),
            pltpu.VMEM((n_sp, inner, units), bf16),
            pltpu.VMEM((n_sp, inner, units), bf16),
            pltpu.VMEM((n_sp, units, span), bf16),
            pltpu.VMEM((n_tp, quarter, query_width), bf16),
            pltpu.VMEM((n_tp, quarter, query_width), bf16),
            pltpu.VMEM((quarter, width_all), f32),
            pltpu.VMEM((quarter, width_all), f32),
            pltpu.VMEM((tiles, quarter, width_all), bf16),
            pltpu.VMEM((depth, 2, tiles, quarter, span), bf16),
            pltpu.VMEM((depth, 2, 2 * depth, quarter, span), bf16),
            pltpu.VMEM((depth, 2, depth, quarter, span), bf16),
            pltpu.VMEM((depth, 2, 2, quarter, span), bf16),
            pltpu.VMEM((depth, 2, quarter, span), bf16),
            pltpu.SemaphoreType.DMA((total_sends,)),
            pltpu.SemaphoreType.DMA((total_sends,)),
            pltpu.SemaphoreType.DMA((10,)),
        ],
        compiler_params=pltpu.CompilerParams(
            collective_id=0, has_side_effects=True, vmem_limit_bytes=60 * 1024 * 1024
        ),
    )(
        residual,
        queries,
        key_pairs,
        values,
        lambdas,
        head_gain[None],
        out_weight,
        mixer_gain[None],
        before_gain[None],
        after_gain[None],
        gate_weight,
        up_weight,
        down_in,
    )


def fits(mesh):
    return mesh.shape["tp"] == 4 and mesh.shape["sp"] == 8


def solution(mesh):
    return jax.shard_map(
        one_kernel if fits(mesh) else on_device,
        mesh=mesh,
        in_specs=(
            P(("sp", "tp"), None),
            P("sp", "tp"),
            P("sp", "tp"),
            P("sp", "tp"),
            P("tp"),
            P(),
            P(),
            P(),
            P(),
            P(),
            P("sp", "tp"),
            P("sp", "tp"),
            P("tp", "sp"),
        ),
        out_specs=P(("sp", "tp"), None),
        check_vma=False,
    )
```

time: 124 us -> 114 us (0.919)
  the two profiles are of different devices: /device:TPU:5 before, /device:TPU:0 now
where the time goes in v1:
time: 114 us
  Pallas kernels  112 us (98%)
  local copies, waits for them, and re-layouts  1.67 us (1%)
    pallas_call x1, Pallas kernels, one_kernel(): pl.pallas_call(layer, out_shape=jax.ShapeDtypeStruct(residual.shape, bf16...  112 us

profile of v1, /device:TPU:0, one launch (start us, length us, event | category | flops | bytes accessed | tf_op | source)
XLA Modules:
  0.0 113.7 jit_solution(17087259043666064801)
XLA Ops:
  0.0 112.0 %shard_map.127 = bf16[64,2048]{1,0:T(8,128)(2,1)} custom-call(bf16[64,2048]{1,0:T(8,128)(2,1)} %residual_in.1, bf16[256,256]{1,0:T(8,128)(2,1)} %queries_in.1, bf16[256,128]{1,0:T(8,128)(2,1)} %key_in.1, bf16[256,128]{1,0:T(8,128)(2,1)} %value_in.1, f32[2]{0:T(128)} %lambdas.1, f32[1,128]{1,0:T(1,128)} %bitcast.9, bf16[1024,2048]{1,0:T(8,128)(2,1)} %out_in.1, ...), custom_call_target="tpu_custom_call" | custom-call | tf_op jit(solution)/shard_map/pallas_call | solution.py:630
  112.0 1.7 %copy.15 = bf16[64,2048]{1,0:T(8,128)(2,1)} copy(bf16[64,2048]{1,0:T(8,128)(2,1)} %shard_map.127) | data formatting | bytes 524288
